TPU v7x, 256 devices: a whole 4x4x8 slice. The times are simulated.
256 devices in a mesh: ep: 64 (over z, x, core), tp: 4 (over y).
Axes of the slice: x: 4, y: 4, z: 8, core: 2. Of those that a mesh axis runs over, the one named last changes fastest.
Arguments:
- mix_in: bfloat16 [32768, 2048], P('ep'), may hold values from -6 to 6
- forget_shift: float32 [32768], P('ep'), may hold values from -2.5 to 2.5, as said below
- mix_gain: float32 [2048], replicated, may hold values from 0.1 to 1.9
- w_query: bfloat16 [2048, 1024], P(None, 'tp'), may hold values from -0.125 to 0.125
- w_forget: bfloat16 [2048, 1024], P(None, 'tp'), may hold values from -0.125 to 0.125
- w_value: bfloat16 [2048, 1024], P(None, 'tp'), may hold values from -0.125 to 0.125
- forget_room: float32 [1024], P('tp'), may hold values from 0 to 1, as said below
- head_gain: float32 [1024], P('tp'), may hold values from 0.1 to 1.9
- w_out: bfloat16 [1024, 2048], P('tp'), may hold values from -0.1875 to 0.1875
- moe_in: bfloat16 [16384, 2048], P('ep'), may hold values from -6 to 6
- moe_gain: float32 [2048], replicated, may hold values from 0.1 to 1.9
- expert_choice: int32 [16384, 4], P('ep'), may hold values from 0 to 63, as said below
- route_logit: float32 [16384, 4], P(('ep', 'tp')), may hold values from -6 to 6
- w_exp_gate: bfloat16 [64, 2048, 1024], P('ep', None, 'tp'), may hold values from -0.125 to 0.125
- w_exp_up: bfloat16 [64, 2048, 1024], P('ep', None, 'tp'), may hold values from -0.125 to 0.125
- w_exp_down: bfloat16 [64, 1024, 2048], P('ep', 'tp'), may hold values from -0.1875 to 0.1875
- w_sh_gate: bfloat16 [2048, 512], P(None, 'tp'), may hold values from -0.125 to 0.125
- w_sh_up: bfloat16 [2048, 512], P(None, 'tp'), may hold values from -0.125 to 0.125
- w_sh_down: bfloat16 [512, 2048], P('tp'), may hold values from -0.25 to 0.25
Outputs:
- mixer_out: bfloat16 [32768, 2048], P(('ep', 'tp'))
- moe_out: bfloat16 [16384, 2048], P(('ep', 'tp'))
Inputs may be any that keep to these rules, and one draw needn't show every extreme that they name: `forget_room`: positive and at most 1/6 in every entry. `forget_shift`: constant over each aligned span of 64 positions. `expert_choice`: each row names 4 different experts. In each aligned block of 64 rows no expert is named by more than 6 rows; in every draw one expert is named by exactly 6 rows in every block.
All inputs are finite; a program needn't handle non-finite values.
Results may differ from a plain program's by a relative error of at most 0.02.
Values may be sent and summed in bfloat16 or wider, within the bound.
No kernel may reach another device: no remote copies, remote signals or barrier semaphores. Data moves between devices by JAX's collectives and lax.ppermute only.
A program may use at most 128 MiB of HBM per device.

v0:
```python
import jax
import jax.numpy as jnp
from jax import lax
from jax.sharding import Mesh
from jax.sharding import PartitionSpec as P

HEAD_K = 64
HEAD_V = 64
SPAN = 64
TOP_K = 4
EP = ("ep_0", "ep_1", "ep_2")
EP_TP = ("ep_0", "ep_1", "ep_2", "tp")
epsilon = 1e-06
route_scale = 2.5


def neutral_like(x, identity):
    return jax.tree.map(
        lambda a, e: jnp.broadcast_to(jnp.asarray(e, a.dtype), a.shape), x, identity
    )


def prefix_by_axis(x, axes, combine, identity):
    before = start = neutral_like(x, identity)
    running = x
    for axis in reversed(axes):
        peers, index = (lax.axis_size(axis), lax.axis_index(axis))
        pieces = jax.tree.map(
            lambda part, kind: lax.all_gather(part.astype(kind), axis),
            running,
            (jnp.bfloat16, jnp.bfloat16),
        )
        inside, running = (start, start)
        for k in range(peers):
            passed = k < index
            running = combine(
                running, jax.tree.map(lambda part, own: part[k].astype(own.dtype), pieces, x)
            )
            inside = jax.tree.map(lambda new, old: jnp.where(passed, new, old), running, inside)
        before = combine(inside, before)
    return before


def norm_rows(row_data, gain_vec):
    widened = row_data.astype(jnp.float32)
    scaled = widened * lax.rsqrt(jnp.mean(widened * widened, axis=-1, keepdims=True) + epsilon)
    return (scaled * gain_vec).astype(jnp.bfloat16)


def join_states(earlier, latter):
    return (earlier[0] * latter[0], latter[0][..., None] * earlier[1] + latter[1])


def block_terms(queries, keyed, log_forget, values, span_len):
    token_count, head_count, key_width = queries.shape
    blocks = token_count // span_len
    key_shape = (blocks, span_len, head_count, key_width)
    queries = queries.reshape(key_shape)
    keyed = keyed.reshape(key_shape)
    log_forget = log_forget.reshape(key_shape)
    values = values.reshape(blocks, span_len, head_count, values.shape[-1])
    log_decay = jnp.cumsum(log_forget, axis=1)
    middle = log_decay[:, span_len // 2 : span_len // 2 + 1]
    block_end = log_decay[:, span_len - 1 :]
    scores = jnp.einsum(
        "nthd,nshd->nhts",
        queries * jnp.exp(log_decay - middle),
        keyed * jnp.exp(middle - log_decay),
    )
    causal = jnp.arange(span_len)[:, None] >= jnp.arange(span_len)[None, :]
    scores = jnp.where(causal, scores, 0.0)
    within = jnp.einsum("nhts,nshv->nthv", scores, values)
    query_decay = queries * jnp.exp(log_decay)
    decay_total = jnp.exp(block_end[:, 0])
    state_added = jnp.einsum("nshd,nshv->nhdv", keyed * jnp.exp(block_end - log_decay), values)
    return (within, query_decay, decay_total, state_added)


def local(
    mix_in,
    forget_shift,
    mix_gain,
    w_query,
    w_forget,
    w_value,
    forget_room,
    head_gain,
    w_out,
    moe_in,
    moe_gain,
    expert_choice,
    route_logit,
    w_exp_gate,
    w_exp_up,
    w_exp_down,
    w_sh_gate,
    w_sh_up,
    w_sh_down,
):
    tp_count = lax.axis_size("tp")
    tp_rank = lax.axis_index("tp")
    gate_whole, up_whole, down_whole = (
        lax.all_gather(w_exp_gate, "tp", axis=2, tiled=True),
        lax.all_gather(w_exp_up, "tp", axis=2, tiled=True),
        lax.all_gather(w_exp_down, "tp", axis=1, tiled=True),
    )
    normed = norm_rows(mix_in, mix_gain)
    queries = jax.nn.silu(jnp.dot(normed, w_query, preferred_element_type=jnp.float32))
    before = jnp.dot(normed, w_forget, preferred_element_type=jnp.float32) + forget_shift[:, None]
    values = jnp.dot(normed, w_value, preferred_element_type=jnp.float32)
    forget_rate = forget_room * jax.nn.sigmoid(-before)
    log_forget = jnp.log1p(-forget_rate)
    token_count = normed.shape[0]
    head_count = values.shape[1] // HEAD_V
    key_shape = (token_count, head_count, HEAD_K)
    within, query_decay, decay_total, state_added = block_terms(
        queries.reshape(key_shape),
        forget_rate.reshape(key_shape),
        log_forget.reshape(key_shape),
        values.reshape(token_count, head_count, HEAD_V),
        SPAN,
    )
    run_total, run_added = lax.associative_scan(join_states, (decay_total, state_added), axis=0)
    start_total, start_added = prefix_by_axis(
        (run_total[-1], run_added[-1]),
        EP,
        join_states,
        (jnp.ones_like(run_total[-1]), jnp.zeros_like(run_added[-1])),
    )
    prior_total = jnp.concatenate([jnp.ones_like(run_total[:1]), run_total[:-1]], axis=0)
    prior_added = jnp.concatenate([jnp.zeros_like(run_added[:1]), run_added[:-1]], axis=0)
    state_in = prior_total[..., None] * start_added[None] + prior_added
    mixed = within + jnp.einsum("nthd,nhdv->nthv", query_decay, state_in)
    mixed = mixed.reshape(token_count, head_count, HEAD_V)
    normal = mixed * lax.rsqrt(jnp.mean(mixed * mixed, axis=-1, keepdims=True) + epsilon)
    head_out = (normal * head_gain.reshape(head_count, HEAD_V)).astype(jnp.bfloat16)
    mixer_part = jnp.dot(
        head_out.reshape(token_count, head_count * HEAD_V),
        w_out,
        preferred_element_type=jnp.float32,
    )
    row_count = moe_in.shape[0]
    model_width = moe_in.shape[1]
    quarter = row_count // tp_count
    experts = lax.axis_size(EP) * w_exp_gate.shape[0]
    mean_load = quarter * TOP_K // experts
    capacity = mean_load + mean_load // 2
    hidden = norm_rows(moe_in, moe_gain)
    labels = expert_choice.reshape(tp_count, quarter * TOP_K)
    onehot = (labels[..., None] == jnp.arange(experts, dtype=jnp.int32)).astype(jnp.int32)
    places = jnp.sum(jnp.cumsum(onehot, axis=1) * onehot, axis=-1) - 1
    slot_ids = labels * capacity + places
    own_slots = lax.dynamic_index_in_dim(slot_ids, tp_rank, 0, keepdims=False)
    padded = jnp.concatenate([hidden, jnp.zeros((1, model_width), jnp.bfloat16)], axis=0)
    own_tokens = tp_rank * quarter + jnp.arange(quarter * TOP_K) // TOP_K
    own_source = jnp.full((experts * capacity,), row_count, jnp.int32).at[own_slots].set(own_tokens)
    outgoing = padded[own_source].reshape(1, experts, capacity, model_width)
    group_width = gate_whole.shape[2] // tp_count
    down_groups = down_whole[0].reshape(tp_count, group_width, model_width)
    arrived = lax.all_to_all(outgoing, EP, split_axis=1, concat_axis=1, tiled=True)
    gate_pre = jnp.einsum(
        "qecd,df->qecf", arrived, gate_whole[0], preferred_element_type=jnp.float32
    )
    up_pre = jnp.einsum("qecd,df->qecf", arrived, up_whole[0], preferred_element_type=jnp.float32)
    activations = (jax.nn.silu(gate_pre) * up_pre).astype(jnp.bfloat16)
    grouped = activations.reshape(activations.shape[:3] + (tp_count, group_width))
    partial_value = jnp.einsum(
        "qecgf,gfd->qecgd", grouped, down_groups, preferred_element_type=jnp.float32
    )
    summed = jnp.sum(partial_value.astype(jnp.bfloat16).astype(jnp.float32), axis=3)
    results = lax.all_to_all(
        summed.astype(jnp.bfloat16), EP, split_axis=1, concat_axis=1, tiled=True
    )
    returned_rows = results.reshape(experts * capacity, model_width)
    picked = returned_rows[own_slots].reshape(quarter, TOP_K, model_width).astype(jnp.float32)
    chance = jax.nn.sigmoid(route_logit)
    weights = chance / jnp.sum(chance, axis=-1, keepdims=True) * route_scale
    routed = jnp.sum(weights[..., None] * picked, axis=1)
    shared_gate = jnp.dot(hidden, w_sh_gate, preferred_element_type=jnp.float32)
    shared_up = jnp.dot(hidden, w_sh_up, preferred_element_type=jnp.float32)
    shared_act = (jax.nn.silu(shared_gate) * shared_up).astype(jnp.bfloat16)
    shared_part = jnp.dot(shared_act, w_sh_down, preferred_element_type=jnp.float32)
    mixer_sum, shared_sum = (
        lax.psum_scatter(
            mixer_part.astype(jnp.bfloat16), "tp", scatter_dimension=0, tiled=True
        ).astype(jnp.float32),
        lax.psum_scatter(
            shared_part.astype(jnp.bfloat16), "tp", scatter_dimension=0, tiled=True
        ).astype(jnp.float32),
    )
    return (mixer_sum.astype(jnp.bfloat16), (routed + shared_sum).astype(jnp.bfloat16))


def solution(mesh):
    finer = Mesh(mesh.devices.reshape(8, 4, 2, mesh.shape["tp"]), ("ep_0", "ep_1", "ep_2", "tp"))
    in_specs = (
        P(EP, None),
        P(EP),
        P(),
        P(None, "tp"),
        P(None, "tp"),
        P(None, "tp"),
        P("tp"),
        P("tp"),
        P("tp", None),
        P(EP, None),
        P(),
        P(EP, None),
        P(EP_TP, None),
        P(EP, None, "tp"),
        P(EP, None, "tp"),
        P(EP, "tp", None),
        P(None, "tp"),
        P(None, "tp"),
        P("tp", None),
    )
    out_specs = (P(EP_TP, None), P(EP_TP, None))
    return jax.shard_map(local, mesh=finer, in_specs=in_specs, out_specs=out_specs, check_vma=False)
```

profile of v0, /device:TPU:2, one launch (start us, length us, event | category | flops | bytes accessed | tf_op | source)
XLA Modules:
  0.0 262.9 jit_solution(2775184898795424189)
XLA Ops:
  7.2 0.7 all-gather.4.cloned.1.call-update
  8.0 0.7 all-gather.6.cloned.1.call-update
  8.7 0.7 all-gather.8.cloned.1.call-update
  9.9 2.4 reduce-window.6
  12.6 0.3 fusion.7
  12.9 0.3 fusion.9
  13.5 1.4 scatter_custom_fusion
  14.9 3.1 %gather_fusion = bf16[384,2048]{1,0:T(8,128)(2,1)} fusion(bf16[257,2048]{1,0:T(8,128)(2,1)S(1)} %concatenate.27, s32[1024]{0:T(1024)S(1)} %pad_clamp_fusion.1), kind=kCustom, calls=%fused_computation | custom fusion | bytes 3147264 | tf_op jit(solution)/shard_map/gather | solution.py:157
  18.1 3.7 %reshape.273 = bf16[1,64,6,2048]{3,2,1,0:T(8,128)(2,1)} reshape(bf16[384,2048]{1,0:T(8,128)(2,1)} %gather_fusion) | data formatting | bytes 3145728 | tf_op jit(solution)/shard_map/reshape | solution.py:157
  21.7 12.3 %all-to-all-start = ((bf16[1,64,6,2048]{3,2,0,1:T(8,128)(2,1)}), bf16[1,64,6,2048]{3,2,0,1:T(8,128)(2,1)}, u32[]{:S(2)}, u32[]{:S(2)}) async-start(bf16[1,64,6,2048]{3,2,0,1:T(8,128)(2,1)} %bitcast.171), calls=%async_computation.1 | async-start | bytes 4194304 | tf_op jit(solution)/shard_map/all_to_all | solution.py:160
  34.1 1.5 fusion.107
  35.6 1.8 convolution_convert_fusion.1
  37.5 2.2 fusion
  39.9 1.9 negate_log-plus-one_fusion
  41.8 2.6 reshape_reshape.14
  44.4 1.3 fusion.32
  46.1 0.6 add_multiply_fusion.1
  46.7 0.6 copy.132
  47.4 2.0 all_gather.33
  49.3 0.5 fusion.73
  49.9 0.6 convert_bitcast_fusion.4
  50.4 1.4 reshape_reshape.15
  51.8 2.6 %divide_multiply_fusion = f32[512,256]{1,0:T(8,128)S(1)} fusion(bf16[2048,256]{1,0:T(8,128)(2,1)} %param.22, bf16[512,2048]{1,0:T(8,128)(2,1)} %param.19, f32[2048]{0:T(1024)S(1)} %copy-done.30, f32[512]{0:T(512)S(1)} %add_rsqrt_fusion), kind=kOutput, calls=%fused_computation.66 | convolution fusion | flops 541589504 | bytes 3680256 | tf_op jit(solution)/shard_map/dot_general | solution.py:108
  54.5 1.5 reshape_reshape.13
  56.0 2.7 %fusion.99 = bf16[512,256]{1,0:T(8,128)(2,1)S(1)} fusion(bf16[2048,256]{1,0:T(8,128)(2,1)} %param.24, bf16[512,2048]{1,0:T(8,128)(2,1)} %param.19, f32[2048]{0:T(1024)S(1)} %copy-done.30, f32[512]{0:T(512)S(1)} %add_rsqrt_fusion), kind=kOutput, calls=%fused_computation.183 | convolution fusion | flops 541065216 | bytes 3418112 | tf_op jit(solution)/shard_map/dot_general | solution.py:110
  58.7 0.2 reshape_reshape.12
  58.9 4.2 %exponential_multiply_fusion = (bf16[8,64,4,64]{3,0,1,2:T(8,128)(2,1)}, bf16[8,64,4,64]{3,0,1,2:T(8,128)(2,1)}, bf16[8,64,4,64]{3,0,1,2:T(8,128)(2,1)}, bf16[8,64,4,64]{3,0,1,2:T(8,128)(2,1)S(1)}) fusion(f32[8,64,4,64]{3,0,1,2:T(8,128)S(1)} %fusion.32, f32[8,64,4,64]{3,2,1,0:T(4,128)} %reshape_reshape.13, f32[8,4,64]{2,0,1:T(8,128)S(1)} %get-tuple-element.11, ...), kind=kLoop, calls=%fused_computation.45 | loop fusion | flops 1441792 | bytes 2637824 | tf_op jit(solution)/shard_map/mul | solution.py:73
  63.1 0.3 fusion.26
  64.0 0.7 pad_maximum_fusion.1
  64.8 3.1 %pad.49 = f32[4,4,64,64]{3,2,1,0:T(8,128)S(1)} pad(f32[2,4,64,64]{3,2,1,0:T(8,128)} %pad_maximum_fusion.1, f32[]{:T(128)} %constant.32.clone.1), padding=0_1_1x0_0_0x0_0_0x0_0_0 | pad | bytes 393220 | tf_op jit(solution)/shard_map/pad | solution.py:123
  67.9 3.2 %pad.50 = f32[4,4,64,64]{3,2,1,0:T(8,128)} pad(f32[2,4,64,64]{3,2,1,0:T(8,128)S(1)} %pad_add_fusion, f32[]{:T(128)} %constant.32.clone.1), padding=1_0_1x0_0_0x0_0_0x0_0_0 | pad | bytes 393220 | tf_op jit(solution)/shard_map/pad | solution.py:123
  71.1 1.9 add.256
  73.0 9.2 %pad.101 = f32[8,4,64,64]{3,2,1,0:T(8,128)} pad(f32[4,4,64,64]{3,2,1,0:T(8,128)} %add.256, f32[]{:T(128)} %constant.32.clone.1), padding=1_0_1x0_0_0x0_0_0x0_0_0 | pad | bytes 786436
  82.3 1.2 fusion.47
  83.5 0.2 pad.51
  83.7 0.9 add_convert_fusion.1
  84.7 1.9 all_gather.36
  86.6 7.8 %all_gather.34 = bf16[4,4,64]{2,1,0:T(4,128)(2,1)S(1)} all-gather(bf16[1,4,64]{2,1,0:T(4,128)(2,1)S(1)} %copy-done.27), channel_id=1, replica_groups=mesh['ep_0'=8,'ep_1'=4,'ep_2'=2,'tp'=4] {'ep_1'}, dimensions={0}, use_global_device_ids=true | all-gather | bytes 2560 | tf_op jit(solution)/shard_map/all_gather | solution.py:29
  94.4 0.6 fusion.77
  95.1 0.4 copy-done.17
  95.7 17.1 %all_gather.35 = bf16[8,4,64]{2,1,0:T(4,128)(2,1)} all-gather(bf16[1,4,64]{2,1,0:T(4,128)(2,1)S(1)} %fusion.78), channel_id=1, replica_groups=mesh['ep_0'=8,'ep_1'=4,'ep_2'=2,'tp'=4] {'ep_0'}, dimensions={0}, use_global_device_ids=true | all-gather | bytes 4608 | tf_op jit(solution)/shard_map/all_gather | solution.py:29
  112.7 11.6 %all_gather.37 = bf16[4,4,64,64]{3,2,1,0:T(8,128)(2,1)S(1)} all-gather(bf16[1,4,64,64]{3,2,1,0:T(8,128)(2,1)S(1)} %fusion.60), channel_id=1, replica_groups=mesh['ep_0'=8,'ep_1'=4,'ep_2'=2,'tp'=4] {'ep_1'}, dimensions={0}, use_global_device_ids=true | all-gather | bytes 163840 | tf_op jit(solution)/shard_map/all_gather | solution.py:29
  124.4 0.6 iota_compare_fusion.2
  125.0 0.2 fusion.59
  125.2 27.5 %all_gather.38 = bf16[8,4,64,64]{3,2,1,0:T(8,128)(2,1)} all-gather(bf16[1,4,64,64]{3,2,1,0:T(8,128)(2,1)S(1)} %fusion.59), channel_id=1, replica_groups=mesh['ep_0'=8,'ep_1'=4,'ep_2'=2,'tp'=4] {'ep_0'}, dimensions={0}, use_global_device_ids=true | all-gather | bytes 294912 | tf_op jit(solution)/shard_map/all_gather | solution.py:29
  153.0 2.3 add_bitcast_fusion.1
  155.3 1.9 fusion.17
  157.2 1.4 slice_add_fusion.4
  158.6 1.2 multiply_reduce_fusion.1
  159.9 0.6 copy.138
  160.5 0.3 reshape.270
  161.0 2.1 convolution_convert_fusion
  163.1 5.1 %fusion.5 = f32[64,6,1024]{2,0,1:T(8,128)S(1)} fusion(bf16[1,2048,1024]{2,1,0:T(8,128)(2,1)} %all-gather.4.cloned.1.call-done, bf16[1,64,6,2048]{3,2,0,1:T(8,128)(2,1)} %all-to-all-done), kind=kOutput, calls=%fused_computation.11 | convolution fusion | flops 1610612736 | bytes 7340032 | tf_op jit(solution)/shard_map/qecd,df->qecf/dot_general | solution.py:161
  168.3 5.1 %multiply_convert_fusion = bf16[64,6,1024]{2,0,1:T(8,128)(2,1)S(1)} fusion(f32[64,6,1024]{2,0,1:T(8,128)S(1)} %fusion.5, bf16[1,2048,1024]{2,1,0:T(8,128)(2,1)} %all-gather.6.cloned.1.call-done, bf16[1,64,6,2048]{3,2,0,1:T(8,128)(2,1)} %all-to-all-done), kind=kOutput, calls=%fused_computation.23 | convolution fusion | flops 1612972032 | bytes 8126464 | tf_op jit(solution)/shard_map/qecd,df->qecf/dot_general | solution.py:164
  173.4 3.6 %all-gather.8.cloned.1.call-done = bf16[1,1024,2048]{2,1,0:T(8,128)(2,1)} async-done(((bf16[1,256,2048]{2,1,0:T(8,128)(2,1)}), bf16[1,1024,2048]{2,1,0:T(8,128)(2,1)}) %all-gather.8.cloned.1.call-update) | async-done | bytes 4194320 | tf_op jit(solution)/shard_map/all_gather | solution.py:105
  177.1 4.1 %convert_reduce_fusion = bf16[64,6,2048]{2,0,1:T(8,128)(2,1)S(1)} fusion(bf16[4,256,2048,1]{2,1,3,0:T(8,128)(2,1)} %bitcast.177, bf16[6,8,4,8,256]{4,3,2,1,0:T(8,128)(2,1)S(1)} %bitcast.178), kind=kOutput, calls=%fused_computation.3 | convolution fusion | flops 1616117760 | bytes 6553600 | tf_op jit(solution)/shard_map/qecgf,gfd->qecgd/dot_general | solution.py:167
  181.2 2.2 copy.149
  183.4 10.9 %all-to-all-start.1 = ((bf16[1,64,6,2048]{3,2,0,1:T(8,128)(2,1)}), bf16[1,64,6,2048]{3,2,0,1:T(8,128)(2,1)}, u32[]{:S(2)}, u32[]{:S(2)}) async-start(bf16[1,64,6,2048]{3,2,0,1:T(8,128)(2,1)} %copy.149), calls=%async_computation.2 | async-start | bytes 4194304 | tf_op jit(solution)/shard_map/all_to_all | solution.py:171
  194.5 51.0 %all-to-all-done.1 = bf16[1,64,6,2048]{3,2,0,1:T(8,128)(2,1)} async-done(((bf16[1,64,6,2048]{3,2,0,1:T(8,128)(2,1)}), bf16[1,64,6,2048]{3,2,0,1:T(8,128)(2,1)}, u32[]{:S(2)}, u32[]{:S(2)}) %all-to-all-start.1) | async-done | bytes 1572896 | tf_op jit(solution)/shard_map/all_to_all | solution.py:171
  245.4 2.6 reshape.276
  248.0 2.4 gather_fusion.1
  250.4 1.7 reshape.290
  252.1 2.3 multiply_reduce_fusion
  254.5 1.9 add_convert_fusion
  (143 shorter events, 3.3 us)
Async XLA Ops:
  7.2 153.8 %copy-start = (bf16[256,2048]{1,0:T(8,128)(2,1)S(1)}, bf16[256,2048]{1,0:T(8,128)(2,1)}, u32[]{:S(2)}) copy-start(bf16[256,2048]{1,0:T(8,128)(2,1)} %param.27) | copy-start | bytes 3145732
  7.2 2.3 copy-start.24
  7.2 155.9 %all-gather.4.cloned.1.call-start = ((), (), s32[]{:S(2)}) async-start(), calls=%async_computation.5 | async-start | bytes 5242880 | tf_op jit(solution)/shard_map/all_gather | solution.py:103
  7.9 4.6 %copy-start.1 = (bf16[256,2048]{1,0:T(8,128)(2,1)S(1)}, bf16[256,2048]{1,0:T(8,128)(2,1)}, u32[]{:S(2)}) copy-start(bf16[256,2048]{1,0:T(8,128)(2,1)} %param.28) | copy-start | bytes 3145732
  7.9 160.4 %all-gather.6.cloned.1.call-start = ((), (), s32[]{:S(2)}) async-start(), calls=%async_computation.6 | async-start | bytes 5242880 | tf_op jit(solution)/shard_map/all_gather | solution.py:104
  8.7 4.2 %copy-start.20 = (f32[2048]{0:T(1024)S(1)}, f32[2048]{0:T(1024)}, u32[]{:S(2)}) copy-start(f32[2048]{0:T(1024)} %param.29) | copy-start | bytes 24580
  8.7 168.4 %all-gather.8.cloned.1.call-start = ((), (), s32[]{:S(2)}) async-start(), calls=%async_computation.7 | async-start | bytes 5242880 | tf_op jit(solution)/shard_map/all_gather | solution.py:105
  13.5 4.6 %copy-start.25 = (s32[256,1]{0,1:T(1,128)}, s32[256,1]{0,1:T(1,128)S(1)}, u32[]{:S(2)}) copy-start(s32[256,1]{0,1:T(1,128)S(1)} %compare_select_fusion) | copy-start | bytes 3076
  21.7 13.9 %copy-start.4 = (bf16[128,2048]{1,0:T(8,128)(2,1)S(1)}, bf16[128,2048]{1,0:T(8,128)(2,1)}, u32[]{:S(2)}) copy-start(bf16[128,2048]{1,0:T(8,128)(2,1)} %param.37) | copy-start | bytes 1572868
  21.7 13.9 %copy-start.5 = (bf16[2048,128]{1,0:T(8,128)(2,1)S(1)}, bf16[2048,128]{1,0:T(8,128)(2,1)}, u32[]{:S(2)}) copy-start(bf16[2048,128]{1,0:T(8,128)(2,1)} %param.36) | copy-start | bytes 1572868
  21.7 141.3 %all-to-all-start = ((bf16[1,64,6,2048]{3,2,0,1:T(8,128)(2,1)}), bf16[1,64,6,2048]{3,2,0,1:T(8,128)(2,1)}, u32[]{:S(2)}, u32[]{:S(2)}) async-start(bf16[1,64,6,2048]{3,2,0,1:T(8,128)(2,1)} %bitcast.171), calls=%async_computation.1 | async-start | bytes 4194304 | tf_op jit(solution)/shard_map/all_to_all | solution.py:160
  34.1 220.4 %reduce-scatter.5.cloned.1.call-start = ((), (), s32[]{:S(2)}) async-start(), calls=%async_computation.8 | async-start | bytes 1310720 | tf_op jit(solution)/shard_map/reduce_scatter | solution.py:187
  35.6 4.1 %copy-start.31 = (f32[512]{0:T(512)S(1)}, f32[512]{0:T(512)}, u32[]{:S(2)}) copy-start(f32[512]{0:T(512)} %param.20) | copy-start | bytes 6148
  37.4 2.3 copy-start.3
  37.4 2.3 copy-start.30
  37.4 2.4 copy-start.32
  37.5 218.9 %reduce-scatter.3.cloned.1.call-start = ((), (), s32[]{:S(2)}) async-start(), calls=%async_computation.4 | async-start | bytes 2621440 | tf_op jit(solution)/shard_map/reduce_scatter | solution.py:184
  37.5 2.4 copy-start.29
  41.8 8.6 %copy-start.6 = (f32[512,256]{1,0:T(8,128)S(1)}, f32[512,256]{1,0:T(8,128)}, u32[]{:S(2)}) copy-start(f32[512,256]{1,0:T(8,128)} %get-tuple-element.35) | copy-start | bytes 1572868
  45.8 8.7 %copy-start.8 = (f32[8,4,64]{2,0,1:T(8,128)}, f32[8,4,64]{2,0,1:T(8,128)S(1)}, u32[]{:S(2)}) copy-start(f32[8,4,64]{2,0,1:T(8,128)S(1)} %fusion.95) | copy-start | bytes 24580
  46.1 8.4 %copy-start.9 = (f32[4,4,64]{2,0,1:T(4,128)}, f32[4,4,64]{2,0,1:T(4,128)S(1)}, u32[]{:S(2)}) copy-start(f32[4,4,64]{2,0,1:T(4,128)S(1)} %add.249) | copy-start | bytes 12292
  49.3 5.2 %copy-start.13 = (bf16[2,4,64]{2,1,0:T(4,128)(2,1)}, bf16[2,4,64]{2,1,0:T(4,128)(2,1)S(1)}, u32[]{:S(2)}) copy-start(bf16[2,4,64]{2,1,0:T(4,128)(2,1)S(1)} %all_gather.33) | copy-start | bytes 3076
  67.9 14.3 %copy-start.15 = (f32[3,4,64]{2,1,0:T(4,128)S(1)}, f32[3,4,64]{2,1,0:T(4,128)}, u32[]{:S(2)}) copy-start(f32[3,4,64]{2,1,0:T(4,128)} %copy.132) | copy-start | bytes 9220
  82.2 4.4 %copy-start.27 = (bf16[1,4,64]{2,1,0:T(4,128)(2,1)S(1)}, bf16[1,4,64]{2,1,0:T(4,128)(2,1)}, u32[]{:S(2)}) copy-start(bf16[1,4,64]{2,1,0:T(4,128)(2,1)} %fusion.73) | copy-start | bytes 1540
  82.2 12.2 %copy-start.14 = (bf16[2,4,64]{2,1,0:T(4,128)(2,1)S(1)}, bf16[2,4,64]{2,1,0:T(4,128)(2,1)}, u32[]{:S(2)}) copy-start(bf16[2,4,64]{2,1,0:T(4,128)(2,1)} %copy-done.13) | copy-start | bytes 3076
  82.2 12.8 %copy-start.19 = (f32[4,64]{1,0:T(4,128)S(1)}, f32[4,64]{1,0:T(4,128)}, u32[]{:S(2)}) copy-start(f32[4,64]{1,0:T(4,128)} %convert_bitcast_fusion.4) | copy-start | bytes 3076
  82.2 13.4 %slice-start = ((f32[8,4,64]{2,0,1:T(8,128)}), f32[1,4,64]{2,0,1:T(1,128)S(1)}, s32[]{:S(2)}) async-start(f32[8,4,64]{2,0,1:T(8,128)} %copy-done.8), calls=%async_computation.9 | async-start | bytes 4096 | tf_op jit(solution)/shard_map/slice | solution.py:123
  82.2 13.3 %copy-start.11 = (f32[3,4,64]{2,0,1:T(4,128)S(1)}, f32[3,4,64]{2,0,1:T(4,128)}, u32[]{:S(2)}) copy-start(f32[3,4,64]{2,0,1:T(4,128)} %add_multiply_fusion.1) | copy-start | bytes 9220
  82.2 13.4 %copy-start.10 = (f32[4,4,64]{2,0,1:T(4,128)S(1)}, f32[4,4,64]{2,0,1:T(4,128)}, u32[]{:S(2)}) copy-start(f32[4,4,64]{2,0,1:T(4,128)} %copy-done.9) | copy-start | bytes 12292
  95.0 0.6 copy-start.17
  95.0 30.2 %copy-start.16 = (f32[4,64]{1,0:T(4,128)}, f32[4,64]{1,0:T(4,128)S(1)}, u32[]{:S(2)}) copy-start(f32[4,64]{1,0:T(4,128)S(1)} %get-tuple-element.26) | copy-start | bytes 3076
  124.4 28.6 %copy-start.12 = (bf16[8,4,64]{2,1,0:T(4,128)(2,1)S(1)}, bf16[8,4,64]{2,1,0:T(4,128)(2,1)}, u32[]{:S(2)}) copy-start(bf16[8,4,64]{2,1,0:T(4,128)(2,1)} %all_gather.35) | copy-start | bytes 12292
  124.4 28.6 %copy-start.18 = (f32[4,64]{1,0:T(4,128)S(1)}, f32[4,64]{1,0:T(4,128)}, u32[]{:S(2)}) copy-start(f32[4,64]{1,0:T(4,128)} %copy-done.17) | copy-start | bytes 3076
  124.4 28.6 %copy-start.21 = (f32[4,64]{1,0:T(4,128)S(1)}, f32[4,64]{1,0:T(4,128)}, u32[]{:S(2)}) copy-start(f32[4,64]{1,0:T(4,128)} %get-tuple-element.2) | copy-start | bytes 3076
  124.4 28.6 %copy-start.22 = (f32[4,64]{1,0:T(4,128)S(1)}, f32[4,64]{1,0:T(4,128)}, u32[]{:S(2)}) copy-start(f32[4,64]{1,0:T(4,128)} %get-tuple-element.3) | copy-start | bytes 3076
  157.2 1.4 copy-start.2
  157.2 1.4 copy-start.7
  159.9 1.0 copy-start.28
  183.4 10.9 %copy-start.23 = (f32[64,4]{0,1:T(4,128)S(1)}, f32[64,4]{0,1:T(4,128)}, u32[]{:S(2)}) copy-start(f32[64,4]{0,1:T(4,128)} %param.31) | copy-start | bytes 3076
  183.4 11.0 %copy-start.26 = (s32[256,1]{0,1:T(1,128)S(1)}, s32[256,1]{0,1:T(1,128)}, u32[]{:S(2)}) copy-start(s32[256,1]{0,1:T(1,128)} %copy-done.25) | copy-start | bytes 3076
  183.4 62.0 %all-to-all-start.1 = ((bf16[1,64,6,2048]{3,2,0,1:T(8,128)(2,1)}), bf16[1,64,6,2048]{3,2,0,1:T(8,128)(2,1)}, u32[]{:S(2)}, u32[]{:S(2)}) async-start(bf16[1,64,6,2048]{3,2,0,1:T(8,128)(2,1)} %copy.149), calls=%async_computation.2 | async-start | bytes 4194304 | tf_op jit(solution)/shard_map/all_to_all | solution.py:171
Sparse Core Ops, SparseCore 0:
  9.8 56.9 all-gather.3
  68.6 54.8 all-gather.5
  125.3 51.7 all-gather.7
  179.5 26.6 reduce-scatter.4
  209.1 32.0 reduce-scatter.2
where the time goes:
time: 265 us; the launch traced here: 263 us
  blocking collectives  67.9 us (26%)
  waiting for transfers between devices  56.7 us (21%)
  local copies, waits for them, and re-layouts  42.2 us (16%)
  matrix products  30.4 us (11%)
  other arithmetic  27.6 us (10%)
  starting transfers between devices  23.4 us (9%)
  between operations  14.6 us (6%)
    all_gather x6, blocking collectives, prefix_by_axis(): lax.all_gather(part.astype(kind), axis)  67.9 us
    all_to_all x1, waiting for transfers between devices, local(): lax.all_to_all(summed.astype(jnp.bfloat16), EP, split_axis=1, concat_axis...  51 us
    all_to_all x1, starting transfers between devices, local(): lax.all_to_all(outgoing, EP, split_axis=1, concat_axis=1, tiled=True)  12.3 us
    all_to_all x1, starting transfers between devices, local(): lax.all_to_all(summed.astype(jnp.bfloat16), EP, split_axis=1, concat_axis...  10.9 us
    unnamed x70, local copies, waits for them, and re-layouts  10.1 us
    pad x7, local copies, waits for them, and re-layouts, local(): lax.associative_scan(join_states, (decay_total, state_added), axis=0)  6.75 us
  transfers between devices with their start and end apart: 7, of which 2 were waited for; matrix products, arithmetic and copies ran while one was open for 38% of the time, Pallas kernels for 0%

commit v1 on v0

--- a/solution.py
+++ b/solution.py
@@ -157,7 +157,15 @@
     outgoing = padded[own_source].reshape(1, experts, capacity, model_width)
     group_width = gate_whole.shape[2] // tp_count
     down_groups = down_whole[0].reshape(tp_count, group_width, model_width)
-    arrived = lax.all_to_all(outgoing, EP, split_axis=1, concat_axis=1, tiled=True)
+
+    def register_steps_all(vals):
+        high = lax.axis_size(EP)
+        arr_out = jnp.split(vals, high, axis=1)
+        kept_arr = jnp.stack(arr_out, 0)
+        base_arr = lax.all_to_all(kept_arr, EP, 0, 0)
+        return jnp.concatenate(base_arr, 1)
+
+    arrived = register_steps_all(outgoing)
     gate_pre = jnp.einsum(
         "qecd,df->qecf", arrived, gate_whole[0], preferred_element_type=jnp.float32
     )

time: 265 us -> 351 us (1.32); the launches traced: 263 us -> 345 us
  local copies, waits for them, and re-layouts: 42.2 us -> 129 us
  waiting for transfers between devices: 56.7 us -> 53.1 us
    unnamed x70 -> x133, local copies, waits for them, and re-layouts: 10.1 us -> 95.9 us
    all_gather x1, waiting for transfers between devices: 3.63 us -> 0.02 us  [local(): lax.all_gather(w_exp_down, 'tp', axis=1, tiled=True)]
  transfers between devices with their start and end apart: 7 -> 7, of which waited for: 2 -> 1; matrix products, arithmetic and copies ran while one was open for 38% -> 54% of each run, Pallas kernels for 0% -> 0%
where the time goes in v1:
time: 351 us; the launch traced here: 345 us
  local copies, waits for them, and re-layouts  129 us (37%)
  blocking collectives  67.7 us (19%)
  waiting for transfers between devices  53.1 us (15%)
  matrix products  30.8 us (9%)
  other arithmetic  27.6 us (8%)
  starting transfers between devices  21.5 us (6%)
  between operations  14.6 us (4%)
    unnamed x133, local copies, waits for them, and re-layouts  95.9 us
    all_gather x6, blocking collectives, prefix_by_axis(): lax.all_gather(part.astype(kind), axis)  67.7 us
    all_to_all x1, waiting for transfers between devices, local(): lax.all_to_all(summed.astype(jnp.bfloat16), EP, split_axis=1, concat_axis...  51 us
    all_to_all x1, starting transfers between devices, register_steps_all(): base_arr = lax.all_to_all(kept_arr, EP, 0, 0)  12.3 us
    all_to_all x1, starting transfers between devices, local(): lax.all_to_all(summed.astype(jnp.bfloat16), EP, split_axis=1, concat_axis...  8.98 us
  transfers between devices with their start and end apart: 7, of which 1 were waited for; matrix products, arithmetic and copies ran while one was open for 54% of the time, Pallas kernels for 0%

profile of v1, /device:TPU:2, one launch (start us, length us, event | category | flops | bytes accessed | tf_op | source)
XLA Modules:
  0.0 344.7 jit_solution(12743626344734556428)
XLA Ops:
  9.9 2.4 reduce-window.6
  12.8 1.4 scatter_custom_fusion
  14.9 3.1 gather_fusion
  18.1 3.7 %reshape.276 = bf16[1,64,6,2048]{3,2,1,0:T(8,128)(2,1)} reshape(bf16[384,2048]{1,0:T(8,128)(2,1)} %gather_fusion) | data formatting | bytes 3145728 | tf_op jit(solution)/shard_map/reshape | solution.py:157
  23.1 1.4 constant_dynamic-update-slice_fusion.62
  24.5 1.4 constant_dynamic-update-slice_fusion.61
  25.9 1.4 constant_dynamic-update-slice_fusion.60
  28.6 1.4 constant_dynamic-update-slice_fusion.58
  31.3 1.4 constant_dynamic-update-slice_fusion.56
  43.6 1.4 constant_dynamic-update-slice_fusion.47
  45.0 1.4 constant_dynamic-update-slice_fusion.46
  47.7 1.4 constant_dynamic-update-slice_fusion.44
  49.1 1.4 constant_dynamic-update-slice_fusion.43
  53.1 1.4 constant_dynamic-update-slice_fusion.40
  55.9 1.4 constant_dynamic-update-slice_fusion.38
  61.3 1.4 constant_dynamic-update-slice_fusion.34
  64.1 1.4 constant_dynamic-update-slice_fusion.32
  72.2 1.4 constant_dynamic-update-slice_fusion.26
  74.9 1.4 constant_dynamic-update-slice_fusion.24
  77.7 1.4 constant_dynamic-update-slice_fusion.22
  80.4 1.4 constant_dynamic-update-slice_fusion.20
  81.8 1.4 constant_dynamic-update-slice_fusion.19
  83.1 1.4 constant_dynamic-update-slice_fusion.18
  85.8 1.4 constant_dynamic-update-slice_fusion.16
  88.6 1.4 constant_dynamic-update-slice_fusion.14
  91.3 1.4 constant_dynamic-update-slice_fusion.12
  99.5 1.4 constant_dynamic-update-slice_fusion.6
  102.2 1.4 constant_dynamic-update-slice_fusion.4
  107.6 1.4 constant_dynamic-update-slice_fusion
  109.0 12.3 %all-to-all-start = ((bf16[64,1,1,6,2048]{4,3,2,1,0:T(8,128)(2,1)}), bf16[64,1,1,6,2048]{4,3,2,1,0:T(8,128)(2,1)}, u32[]{:S(2)}, u32[]{:S(2)}) async-start(bf16[64,1,1,6,2048]{4,3,2,1,0:T(8,128)(2,1)} %constant_dynamic-update-slice_fusion), calls=%async_computation.1 | async-start | bytes 4194304 | tf_op jit(solution)/shard_map/all_to_all | solution.py:165
  121.4 1.5 fusion.107
  122.9 1.8 convolution_convert_fusion.1
  124.8 2.2 fusion
  127.2 1.9 negate_log-plus-one_fusion
  129.1 2.6 reshape_reshape.14
  134.6 2.0 all_gather.33
  137.7 1.4 reshape_reshape.15
  139.1 2.8 divide_multiply_fusion
  142.0 1.5 reshape_reshape.13
  143.4 2.6 fusion.99
  146.3 4.1 %exponential_multiply_fusion = (bf16[8,64,4,64]{3,0,1,2:T(8,128)(2,1)}, bf16[8,64,4,64]{3,0,1,2:T(8,128)(2,1)}, bf16[8,64,4,64]{3,0,1,2:T(8,128)(2,1)}, bf16[8,64,4,64]{3,0,1,2:T(8,128)(2,1)S(1)}) fusion(f32[8,64,4,64]{3,0,1,2:T(8,128)S(1)} %fusion.32, f32[8,64,4,64]{3,2,1,0:T(4,128)} %reshape_reshape.13, f32[8,4,64]{2,0,1:T(8,128)S(1)} %get-tuple-element.11, ...), kind=kLoop, calls=%fused_computation.45 | loop fusion | flops 1441792 | bytes 2637824 | tf_op jit(solution)/shard_map/mul | solution.py:73
  152.1 3.1 pad.49
  155.2 3.3 pad.50
  158.5 1.9 add.256
  160.4 9.2 %pad.101 = f32[8,4,64,64]{3,2,1,0:T(8,128)} pad(f32[4,4,64,64]{3,2,1,0:T(8,128)} %add.256, f32[]{:T(128)} %constant.32.clone.1), padding=1_0_1x0_0_0x0_0_0x0_0_0 | pad | bytes 786436
  172.0 1.9 all_gather.36
  173.9 7.8 %all_gather.34 = bf16[4,4,64]{2,1,0:T(4,128)(2,1)S(1)} all-gather(bf16[1,4,64]{2,1,0:T(4,128)(2,1)S(1)} %copy-done.27), channel_id=1, replica_groups=mesh['ep_0'=8,'ep_1'=4,'ep_2'=2,'tp'=4] {'ep_1'}, dimensions={0}, use_global_device_ids=true | all-gather | bytes 2560 | tf_op jit(solution)/shard_map/all_gather | solution.py:29
  183.0 16.9 %all_gather.35 = bf16[8,4,64]{2,1,0:T(4,128)(2,1)} all-gather(bf16[1,4,64]{2,1,0:T(4,128)(2,1)S(1)} %fusion.78), channel_id=1, replica_groups=mesh['ep_0'=8,'ep_1'=4,'ep_2'=2,'tp'=4] {'ep_0'}, dimensions={0}, use_global_device_ids=true | all-gather | bytes 4608 | tf_op jit(solution)/shard_map/all_gather | solution.py:29
  199.9 11.4 %all_gather.37 = bf16[4,4,64,64]{3,2,1,0:T(8,128)(2,1)S(1)} all-gather(bf16[1,4,64,64]{3,2,1,0:T(8,128)(2,1)S(1)} %fusion.60), channel_id=1, replica_groups=mesh['ep_0'=8,'ep_1'=4,'ep_2'=2,'tp'=4] {'ep_1'}, dimensions={0}, use_global_device_ids=true | all-gather | bytes 163840 | tf_op jit(solution)/shard_map/all_gather | solution.py:29
  212.1 27.7 %all_gather.38 = bf16[8,4,64,64]{3,2,1,0:T(8,128)(2,1)} all-gather(bf16[1,4,64,64]{3,2,1,0:T(8,128)(2,1)S(1)} %fusion.59), channel_id=1, replica_groups=mesh['ep_0'=8,'ep_1'=4,'ep_2'=2,'tp'=4] {'ep_0'}, dimensions={0}, use_global_device_ids=true | all-gather | bytes 294912 | tf_op jit(solution)/shard_map/all_gather | solution.py:29
  240.1 2.3 add_bitcast_fusion.1
  242.4 1.9 fusion.17
  248.1 2.1 convolution_convert_fusion
  250.2 5.1 %fusion.5 = f32[64,6,1024]{2,0,1:T(8,128)S(1)} fusion(bf16[1,2048,1024]{2,1,0:T(8,128)(2,1)} %all-gather.4.cloned.1.call-done, bf16[64,1,1,6,2048]{4,3,2,1,0:T(8,128)(2,1)} %all-to-all-done), kind=kOutput, calls=%fused_computation.11 | convolution fusion | flops 1610612736 | bytes 7340032 | tf_op jit(solution)/shard_map/qecd,df->qecf/dot_general | solution.py:169
  255.3 5.1 %multiply_convert_fusion = bf16[64,6,1024]{2,0,1:T(8,128)(2,1)S(1)} fusion(f32[64,6,1024]{2,0,1:T(8,128)S(1)} %fusion.5, bf16[1,2048,1024]{2,1,0:T(8,128)(2,1)} %all-gather.6.cloned.1.call-done, bf16[64,1,1,6,2048]{4,3,2,1,0:T(8,128)(2,1)} %all-to-all-done), kind=kOutput, calls=%fused_computation.23 | convolution fusion | flops 1612972032 | bytes 8126464 | tf_op jit(solution)/shard_map/qecd,df->qecf/dot_general | solution.py:172
  260.5 4.5 %convert_reduce_fusion = bf16[64,6,2048]{2,0,1:T(8,128)(2,1)S(1)} fusion(bf16[4,256,2048,1]{2,1,3,0:T(8,128)(2,1)} %bitcast.431, bf16[6,8,4,8,256]{4,3,2,1,0:T(8,128)(2,1)S(1)} %bitcast.432), kind=kOutput, calls=%fused_computation.3 | convolution fusion | flops 1616117760 | bytes 6553600 | tf_op jit(solution)/shard_map/qecgf,gfd->qecgd/dot_general | solution.py:175
  265.0 2.2 copy.299
  267.2 9.0 %all-to-all-start.1 = ((bf16[1,64,6,2048]{3,2,0,1:T(8,128)(2,1)}), bf16[1,64,6,2048]{3,2,0,1:T(8,128)(2,1)}, u32[]{:S(2)}, u32[]{:S(2)}) async-start(bf16[1,64,6,2048]{3,2,0,1:T(8,128)(2,1)} %copy.299), calls=%async_computation.2 | async-start | bytes 4194304 | tf_op jit(solution)/shard_map/all_to_all | solution.py:179
  276.3 51.0 %all-to-all-done.1 = bf16[1,64,6,2048]{3,2,0,1:T(8,128)(2,1)} async-done(((bf16[1,64,6,2048]{3,2,0,1:T(8,128)(2,1)}), bf16[1,64,6,2048]{3,2,0,1:T(8,128)(2,1)}, u32[]{:S(2)}, u32[]{:S(2)}) %all-to-all-start.1) | async-done | bytes 1572896 | tf_op jit(solution)/shard_map/all_to_all | solution.py:179
  327.3 2.6 reshape.279
  329.9 2.4 gather_fusion.1
  332.3 1.7 reshape.293
  334.0 2.3 multiply_reduce_fusion
  336.4 1.9 add_convert_fusion
  (207 shorter events, 71.5 us)
Async XLA Ops:
  7.2 240.9 %copy-start = (bf16[256,2048]{1,0:T(8,128)(2,1)S(1)}, bf16[256,2048]{1,0:T(8,128)(2,1)}, u32[]{:S(2)}) copy-start(bf16[256,2048]{1,0:T(8,128)(2,1)} %param.27) | copy-start | bytes 3145732
  7.2 2.3 copy-start.24
  7.2 243.0 %all-gather.4.cloned.1.call-start = ((), (), s32[]{:S(2)}) async-start(), calls=%async_computation.5 | async-start | bytes 5242880 | tf_op jit(solution)/shard_map/all_gather | solution.py:103
  7.9 6.3 %copy-start.1 = (bf16[256,2048]{1,0:T(8,128)(2,1)S(1)}, bf16[256,2048]{1,0:T(8,128)(2,1)}, u32[]{:S(2)}) copy-start(bf16[256,2048]{1,0:T(8,128)(2,1)} %param.28) | copy-start | bytes 3145732
  7.9 247.3 %all-gather.6.cloned.1.call-start = ((), (), s32[]{:S(2)}) async-start(), calls=%async_computation.6 | async-start | bytes 5242880 | tf_op jit(solution)/shard_map/all_gather | solution.py:104
  8.7 5.8 %copy-start.20 = (f32[2048]{0:T(1024)S(1)}, f32[2048]{0:T(1024)}, u32[]{:S(2)}) copy-start(f32[2048]{0:T(1024)} %param.29) | copy-start | bytes 24580
  8.7 251.8 %all-gather.8.cloned.1.call-start = ((), (), s32[]{:S(2)}) async-start(), calls=%async_computation.7 | async-start | bytes 5242880 | tf_op jit(solution)/shard_map/all_gather | solution.py:105
  12.7 1.7 copy-start.25
  109.0 13.9 %copy-start.4 = (bf16[128,2048]{1,0:T(8,128)(2,1)S(1)}, bf16[128,2048]{1,0:T(8,128)(2,1)}, u32[]{:S(2)}) copy-start(bf16[128,2048]{1,0:T(8,128)(2,1)} %param.37) | copy-start | bytes 1572868
  109.0 13.9 %copy-start.5 = (bf16[2048,128]{1,0:T(8,128)(2,1)S(1)}, bf16[2048,128]{1,0:T(8,128)(2,1)}, u32[]{:S(2)}) copy-start(bf16[2048,128]{1,0:T(8,128)(2,1)} %param.36) | copy-start | bytes 1572868
  109.0 141.1 %all-to-all-start = ((bf16[64,1,1,6,2048]{4,3,2,1,0:T(8,128)(2,1)}), bf16[64,1,1,6,2048]{4,3,2,1,0:T(8,128)(2,1)}, u32[]{:S(2)}, u32[]{:S(2)}) async-start(bf16[64,1,1,6,2048]{4,3,2,1,0:T(8,128)(2,1)} %constant_dynamic-update-slice_fusion), calls=%async_computation.1 | async-start | bytes 4194304 | tf_op jit(solution)/shard_map/all_to_all | solution.py:165
  121.4 215.0 %reduce-scatter.5.cloned.1.call-start = ((), (), s32[]{:S(2)}) async-start(), calls=%async_computation.8 | async-start | bytes 1310720 | tf_op jit(solution)/shard_map/reduce_scatter | solution.py:195
  122.9 4.1 %copy-start.31 = (f32[512]{0:T(512)S(1)}, f32[512]{0:T(512)}, u32[]{:S(2)}) copy-start(f32[512]{0:T(512)} %param.20) | copy-start | bytes 6148
  124.7 2.3 copy-start.3
  124.7 2.3 copy-start.30
  124.7 2.4 copy-start.32
  124.7 213.5 %reduce-scatter.3.cloned.1.call-start = ((), (), s32[]{:S(2)}) async-start(), calls=%async_computation.4 | async-start | bytes 2621440 | tf_op jit(solution)/shard_map/reduce_scatter | solution.py:192
  124.8 2.4 copy-start.29
  129.1 8.6 %copy-start.6 = (f32[512,256]{1,0:T(8,128)S(1)}, f32[512,256]{1,0:T(8,128)}, u32[]{:S(2)}) copy-start(f32[512,256]{1,0:T(8,128)} %get-tuple-element.35) | copy-start | bytes 1572868
  133.0 8.9 %copy-start.8 = (f32[8,4,64]{2,0,1:T(8,128)}, f32[8,4,64]{2,0,1:T(8,128)S(1)}, u32[]{:S(2)}) copy-start(f32[8,4,64]{2,0,1:T(8,128)S(1)} %fusion.95) | copy-start | bytes 24580
  133.4 8.6 %copy-start.9 = (f32[4,4,64]{2,0,1:T(4,128)}, f32[4,4,64]{2,0,1:T(4,128)S(1)}, u32[]{:S(2)}) copy-start(f32[4,4,64]{2,0,1:T(4,128)S(1)} %add.249) | copy-start | bytes 12292
  136.6 5.4 %copy-start.13 = (bf16[2,4,64]{2,1,0:T(4,128)(2,1)}, bf16[2,4,64]{2,1,0:T(4,128)(2,1)S(1)}, u32[]{:S(2)}) copy-start(bf16[2,4,64]{2,1,0:T(4,128)(2,1)S(1)} %all_gather.33) | copy-start | bytes 3076
  155.2 14.4 %copy-start.15 = (f32[3,4,64]{2,1,0:T(4,128)S(1)}, f32[3,4,64]{2,1,0:T(4,128)}, u32[]{:S(2)}) copy-start(f32[3,4,64]{2,1,0:T(4,128)} %copy.283) | copy-start | bytes 9220
  169.6 4.3 %copy-start.27 = (bf16[1,4,64]{2,1,0:T(4,128)(2,1)S(1)}, bf16[1,4,64]{2,1,0:T(4,128)(2,1)}, u32[]{:S(2)}) copy-start(bf16[1,4,64]{2,1,0:T(4,128)(2,1)} %fusion.73) | copy-start | bytes 1540
  169.6 12.1 %copy-start.14 = (bf16[2,4,64]{2,1,0:T(4,128)(2,1)S(1)}, bf16[2,4,64]{2,1,0:T(4,128)(2,1)}, u32[]{:S(2)}) copy-start(bf16[2,4,64]{2,1,0:T(4,128)(2,1)} %copy-done.13) | copy-start | bytes 3076
  169.6 12.7 %copy-start.19 = (f32[4,64]{1,0:T(4,128)S(1)}, f32[4,64]{1,0:T(4,128)}, u32[]{:S(2)}) copy-start(f32[4,64]{1,0:T(4,128)} %convert_bitcast_fusion.4) | copy-start | bytes 3076
  169.6 13.3 %slice-start = ((f32[8,4,64]{2,0,1:T(8,128)}), f32[1,4,64]{2,0,1:T(1,128)S(1)}, s32[]{:S(2)}) async-start(f32[8,4,64]{2,0,1:T(8,128)} %copy-done.8), calls=%async_computation.9 | async-start | bytes 4096 | tf_op jit(solution)/shard_map/slice | solution.py:123
  169.6 13.3 %copy-start.11 = (f32[3,4,64]{2,0,1:T(4,128)S(1)}, f32[3,4,64]{2,0,1:T(4,128)}, u32[]{:S(2)}) copy-start(f32[3,4,64]{2,0,1:T(4,128)} %add_multiply_fusion.1) | copy-start | bytes 9220
  169.6 13.3 %copy-start.10 = (f32[4,4,64]{2,0,1:T(4,128)S(1)}, f32[4,4,64]{2,0,1:T(4,128)}, u32[]{:S(2)}) copy-start(f32[4,4,64]{2,0,1:T(4,128)} %copy-done.9) | copy-start | bytes 12292
  182.3 0.5 copy-start.17
  182.3 29.8 %copy-start.16 = (f32[4,64]{1,0:T(4,128)}, f32[4,64]{1,0:T(4,128)S(1)}, u32[]{:S(2)}) copy-start(f32[4,64]{1,0:T(4,128)S(1)} %get-tuple-element.26) | copy-start | bytes 3076
  211.3 28.8 %copy-start.12 = (bf16[8,4,64]{2,1,0:T(4,128)(2,1)S(1)}, bf16[8,4,64]{2,1,0:T(4,128)(2,1)}, u32[]{:S(2)}) copy-start(bf16[8,4,64]{2,1,0:T(4,128)(2,1)} %all_gather.35) | copy-start | bytes 12292
  211.3 28.8 %copy-start.18 = (f32[4,64]{1,0:T(4,128)S(1)}, f32[4,64]{1,0:T(4,128)}, u32[]{:S(2)}) copy-start(f32[4,64]{1,0:T(4,128)} %copy-done.17) | copy-start | bytes 3076
  211.3 28.8 %copy-start.21 = (f32[4,64]{1,0:T(4,128)S(1)}, f32[4,64]{1,0:T(4,128)}, u32[]{:S(2)}) copy-start(f32[4,64]{1,0:T(4,128)} %get-tuple-element.2) | copy-start | bytes 3076
  211.3 28.8 %copy-start.22 = (f32[4,64]{1,0:T(4,128)S(1)}, f32[4,64]{1,0:T(4,128)}, u32[]{:S(2)}) copy-start(f32[4,64]{1,0:T(4,128)} %get-tuple-element.3) | copy-start | bytes 3076
  244.3 1.4 copy-start.2
  244.3 1.4 copy-start.7
  246.9 1.0 copy-start.28
  267.2 9.0 %copy-start.23 = (f32[64,4]{0,1:T(4,128)S(1)}, f32[64,4]{0,1:T(4,128)}, u32[]{:S(2)}) copy-start(f32[64,4]{0,1:T(4,128)} %param.31) | copy-start | bytes 3076
  267.2 9.1 %copy-start.26 = (s32[256,1]{0,1:T(1,128)S(1)}, s32[256,1]{0,1:T(1,128)}, u32[]{:S(2)}) copy-start(s32[256,1]{0,1:T(1,128)} %copy-done.25) | copy-start | bytes 3076
  267.2 60.1 %all-to-all-start.1 = ((bf16[1,64,6,2048]{3,2,0,1:T(8,128)(2,1)}), bf16[1,64,6,2048]{3,2,0,1:T(8,128)(2,1)}, u32[]{:S(2)}, u32[]{:S(2)}) async-start(bf16[1,64,6,2048]{3,2,0,1:T(8,128)(2,1)} %copy.299), calls=%async_computation.2 | async-start | bytes 4194304 | tf_op jit(solution)/shard_map/all_to_all | solution.py:179
Sparse Core Ops, SparseCore 0:
  9.8 56.9 all-gather.3
  68.6 54.8 all-gather.5
  125.3 51.7 all-gather.7
  179.5 26.6 reduce-scatter.4
  250.3 32.2 reduce-scatter.2
